TPU v7x, 256 devices: a whole 4x4x8 slice. The times are simulated.
256 devices in a mesh: sp: 64 (over z, x, core), tp: 4 (over y).
Axes of the slice: x: 4, y: 4, z: 8, core: 2. Of those that a mesh axis runs over, the one named last changes fastest.
Arguments:
- queries: bfloat16 [32768, 2048], P('sp', 'tp'), may hold values from -90 to 90, as said below
- key_rows: bfloat16 [32768, 512], P('sp', 'tp'), may hold values from -6 to 6
- value_rows: bfloat16 [32768, 512], P('sp', 'tp'), may hold values from -6 to 6
- sink_logits: float32 [16], P('tp'), may hold values from 2 to 7
- residual: bfloat16 [32768, 2048], P('sp'), may hold values from -6 to 6
- norm_gain: float32 [2048], replicated, may hold values from 0.1 to 1.9
- out_weight: bfloat16 [2048, 2048], P('tp'), may hold values from -1.5 to 1.5
- gate_weight: bfloat16 [2048, 5632], P('sp', 'tp'), may hold values from -0.125 to 0.125
- up_weight: bfloat16 [2048, 5632], P('sp', 'tp'), may hold values from -0.125 to 0.125
- down_weight: bfloat16 [5632, 2048], P('tp', 'sp'), may hold values from -0.078125 to 0.078125
Outputs:
- mixed: bfloat16 [32768, 2048], P(('sp', 'tp'))
Inputs may be any that keep to these rules, and one draw needn't show every extreme that they name: queries are mostly of order one; some rows may be much larger.
All inputs are finite; a program needn't handle non-finite values.
Results may differ from a plain program's by a relative error of at most 0.012.
Values may be sent and summed in bfloat16 or wider, within the bound.
A program may use at most 128 MiB of HBM per device.

v0:
```python
import jax
import jax.numpy as jnp
from jax import lax
from jax.sharding import PartitionSpec as P

DH = 128
WIN = 128


EPSILON = 1e-06
MASKED = -1e30


def with_halo(cells, sides, width):
    for axis, dim in sides:
        count = lax.axis_size(axis)
        ends = count - 1
        head = lax.slice_in_dim(cells, 0, width, axis=dim)
        tail = lax.slice_in_dim(cells, cells.shape[dim] - width, cells.shape[dim], axis=dim)
        cells = jnp.concatenate(
            [
                lax.ppermute(tail, axis, [(i, (i + 1) % count) for i in range(ends)]),
                cells,
                lax.ppermute(head, axis, [((i + 1) % count, i) for i in range(ends)]),
            ],
            axis=dim,
        )
    return cells


def split_up(value, dim, size):
    before, after = (value.shape[:dim], value.shape[dim + 1 :])
    return jnp.moveaxis(value.reshape(*before, size, -1, *after), dim, 0)


def sent_and_summed(value, axis, dim):
    size = lax.axis_size(axis)
    blocks = lax.all_to_all(split_up(value, dim, size), axis, 0, 0, tiled=True)
    return jnp.sum(blocks.astype(jnp.float32), axis=0)


def sent_to_all(value, axis):
    size = lax.axis_size(axis)
    return lax.all_to_all(
        jnp.broadcast_to(value[None], (size, *value.shape)), axis, 0, 0, tiled=True
    )


def laid_out(blocks, dim):
    blocks = jnp.moveaxis(blocks, 0, dim)
    lengths = blocks.shape
    return blocks.reshape(*lengths[:dim], lengths[dim] * lengths[dim + 1], *lengths[dim + 2 :])


def gather_directly(value, axis, dim):
    blocks = sent_to_all(value, axis)
    return laid_out(blocks, dim)


def side_by_side(arrays, axis, dim, along):
    ends, at = ([], 0)
    for a in arrays[:-1]:
        at += a.shape[along]
        ends.append(at)
    both = jnp.concatenate(arrays, axis=along)
    return tuple(jnp.split(lax.all_gather(both, axis, axis=dim, tiled=True), ends, axis=along))


def attend_block(query_blk, key_blk, value_blk, sink_logits, query_pos, key_pos, seq_len):
    kv_heads = key_blk.shape[1] // DH
    group_size = query_blk.shape[1] // key_blk.shape[1]
    query_four = query_blk.reshape(query_blk.shape[0], kv_heads, group_size, DH)
    key_three = key_blk.reshape(key_blk.shape[0], kv_heads, DH)
    value_three = value_blk.reshape(value_blk.shape[0], kv_heads, DH)
    scores = jnp.einsum(
        "qhgd,khd->hgqk", query_four, key_three, preferred_element_type=jnp.float32
    ) * DH ** (-0.5)
    allowed = (
        (jnp.abs(key_pos[None, :] - query_pos[:, None]) <= WIN)
        & (key_pos[None, :] >= 0)
        & (key_pos[None, :] < seq_len)
    )
    scores = jnp.where(allowed[None, None], scores, MASKED)
    sink_col = sink_logits.reshape(kv_heads, group_size)[:, :, None]
    highest = jnp.maximum(jnp.max(scores, axis=-1), sink_col)
    weights_exp = jnp.exp(scores - highest[..., None])
    denominator = jnp.sum(weights_exp, axis=-1) + jnp.exp(sink_col - highest)
    probabilities = (weights_exp / denominator[..., None]).astype(jnp.bfloat16)
    heads_out = jnp.einsum(
        "hgqk,khd->qhgd", probabilities, value_three, preferred_element_type=jnp.float32
    )
    return heads_out.astype(jnp.bfloat16).reshape(query_blk.shape[0], kv_heads * group_size * DH)


def rms_scale(rows_wide, norm_gain):
    mean_square = jnp.mean(rows_wide * rows_wide, axis=-1, keepdims=True)
    return (rows_wide * lax.rsqrt(mean_square + EPSILON) * norm_gain).astype(jnp.bfloat16)


def fetch_down(down_weight):
    return lax.all_gather(down_weight, "sp", axis=1, tiled=True)


def shards(
    queries,
    key_rows,
    value_rows,
    sink_logits,
    residual,
    norm_gain,
    out_weight,
    gate_weight,
    up_weight,
    down_weight,
):
    tok_local = queries.shape[0]
    block_len = 2 * WIN
    share_rows = tok_local // lax.axis_size("tp")
    seq_len = tok_local * lax.axis_size("sp")
    device_offset = lax.axis_index("sp") * tok_local
    kv_pair = jnp.stack([key_rows, value_rows])
    kv_ext = with_halo(kv_pair, (("sp", 1),), WIN)

    def one_block(block_index):
        block_first = block_index * block_len
        query_blk = lax.dynamic_slice_in_dim(queries, block_first, block_len, 0)
        key_blk = lax.dynamic_slice_in_dim(kv_ext[0], block_first, block_len + 2 * WIN, 0)
        value_blk = lax.dynamic_slice_in_dim(kv_ext[1], block_first, block_len + 2 * WIN, 0)
        query_pos = device_offset + block_first + jnp.arange(block_len, dtype=jnp.int32)
        key_pos = (
            device_offset + block_first - WIN + jnp.arange(block_len + 2 * WIN, dtype=jnp.int32)
        )
        return attend_block(query_blk, key_blk, value_blk, sink_logits, query_pos, key_pos, seq_len)

    blocks = lax.map(one_block, jnp.arange(tok_local // block_len, dtype=jnp.int32))
    attended = blocks.reshape(tok_local, queries.shape[1])
    own_first = lax.axis_index("tp") * share_rows
    picked = attended
    attn_share = sent_and_summed(
        jnp.dot(picked, out_weight, preferred_element_type=jnp.float32).astype(jnp.bfloat16),
        "tp",
        0,
    )
    middle_own = (
        lax.dynamic_slice_in_dim(residual, own_first, share_rows, 0).astype(jnp.float32)
        + attn_share
    )
    normed_all = gather_directly(rms_scale(middle_own, norm_gain), "tp", 0)
    pieces = side_by_side((gate_weight, up_weight), "sp", 0, 1)
    gate_sectioned = pieces[0]
    up_sectioned = pieces[1]
    gate_acc = jnp.dot(normed_all, gate_sectioned, preferred_element_type=jnp.float32)
    up_acc = jnp.dot(normed_all, up_sectioned, preferred_element_type=jnp.float32)
    down_whole = fetch_down(down_weight)
    hidden = (jax.nn.silu(gate_acc) * up_acc).astype(jnp.bfloat16)
    picked = hidden
    ffn_share = lax.psum_scatter(
        jnp.dot(picked, down_whole, preferred_element_type=jnp.float32).astype(jnp.bfloat16),
        "tp",
        scatter_dimension=0,
        tiled=True,
    ).astype(jnp.float32)
    return (middle_own + ffn_share).astype(jnp.bfloat16)


def solution(mesh):
    placed = (
        P("sp", "tp"),
        P("sp", "tp"),
        P("sp", "tp"),
        P("tp"),
        P("sp", None),
        P(),
        P("tp", None),
        P("sp", "tp"),
        P("sp", "tp"),
        P("tp", "sp"),
    )
    return jax.shard_map(
        shards, mesh=mesh, in_specs=placed, out_specs=P(("sp", "tp"), None), check_vma=False
    )
```

profile of v0, /device:TPU:1, one launch (start us, length us, event | category | flops | bytes accessed | tf_op | source)
XLA Modules:
  0.0 233.1 jit_solution(577112236005821725)
XLA Ops:
  6.5 1.8 pad_maximum_fusion.1
  8.4 0.7 all-gather.5.cloned.1.call-update
  9.1 0.8 pad_maximum_fusion.3
  9.9 4.5 %collective-permute-start = (bf16[2,128,128]{2,1,0:T(8,128)(2,1)S(1)}, bf16[2,128,128]{2,1,0:T(8,128)(2,1)S(1)}, u32[]{:S(2)}, u32[]{:S(2)}) collective-permute-start(bf16[2,128,128]{2,1,0:T(8,128)(2,1)S(1)} %get-tuple-element.122), channel_id=1, source_target_pairs={{0,4},{4,8},{8,12},{12,16},{16,20},{20,24},{24,28},{28,32},{32,36}... | collective-permute-start | bytes 196616 | tf_op jit(solution)/shard_map/ppermute | solution.py:22
  14.4 1.9 collective-permute-start.1
  16.4 3.6 %collective-permute-done.1 = bf16[2,128,128]{2,1,0:T(8,128)(2,1)S(1)} collective-permute-done((bf16[2,128,128]{2,1,0:T(8,128)(2,1)S(1)}, bf16[2,128,128]{2,1,0:T(8,128)(2,1)S(1)}, u32[]{:S(2)}, u32[]{:S(2)}) %collective-permute-start.1) | collective-permute-done | bytes 65568 | tf_op jit(solution)/shard_map/ppermute | solution.py:24
  20.0 1.0 pad_maximum_fusion
  21.0 11.1 %while.12 = (s32[]{:T(128)}, bf16[2,256,512]{2,1,0:T(8,128)(2,1)}, bf16[2,768,128]{2,1,0:T(8,128)(2,1)S(1)}, s32[2]{0:T(128)S(1)}, s32[]{:T(128)}, /*index=5*/bf...) while((s32[]{:T(128)}, bf16[2,256,512]{2,1,0:T(8,128)(2,1)}, ...), condition=%wide.region_3.4_spmd, body=%wide.region_0.3_spmd.sunk | while | flops 273420544 | bytes 14467520 | solution.py:135
  21.0 0.6 dynamic_slice.48
  22.6 1.0 constant_dynamic-slice_fusion.2
  23.7 0.5 fusion.47
  24.3 0.3 fusion.48
  24.7 0.5 convolution_convert_fusion.4
  25.4 0.4 copy-done.4
  25.8 0.8 copy-done.5
  26.6 0.6 dynamic_slice.48
  28.1 1.0 constant_dynamic-slice_fusion.2
  29.3 0.5 fusion.47
  30.2 0.5 convolution_convert_fusion.4
  30.9 0.4 copy-done.4
  31.3 0.8 copy-done.5
  32.1 3.6 %convolution_convert_fusion.1 = bf16[512,2048]{1,0:T(8,128)(2,1)} fusion(bf16[512,512]{1,0:T(8,128)(2,1)} %bitcast.59, bf16[512,2048]{1,0:T(8,128)(2,1)S(1)} %copy-done), kind=kOutput, calls=%fused_computation.30 | convolution fusion | flops 1074790400 | bytes 4718592 | tf_op jit(solution)/shard_map/dot_general | solution.py:140
  35.7 4.4 %all-to-all-start = ((bf16[4,128,2048]{2,1,0:T(8,128)(2,1)}), bf16[4,128,2048]{2,1,0:T(8,128)(2,1)}, u32[]{:S(2)}, u32[]{:S(2)}) async-start(bf16[4,128,2048]{2,1,0:T(8,128)(2,1)} %bitcast.52), calls=%async_computation | async-start | bytes 4194304 | tf_op jit(solution)/shard_map/all_to_all | solution.py:38
  40.2 24.7 %all-to-all-done = bf16[4,128,2048]{2,1,0:T(8,128)(2,1)} async-done(((bf16[4,128,2048]{2,1,0:T(8,128)(2,1)}), bf16[4,128,2048]{2,1,0:T(8,128)(2,1)}, u32[]{:S(2)}, u32[]{:S(2)}) %all-to-all-start) | async-done | bytes 2097184 | tf_op jit(solution)/shard_map/all_to_all | solution.py:38
  64.9 2.2 convert_reduce_fusion
  67.9 30.0 %all_to_all.10 = bf16[4,128,2048]{2,1,0:T(8,128)(2,1)} all-to-all(bf16[4,128,2048]{2,1,0:T(8,128)(2,1)S(1)} %broadcast_in_dim.44), channel_id=1, replica_groups=mesh['sp'=64,'tp'=4] {'tp'}, dimensions={0} | all-to-all | bytes 4194304 | tf_op jit(solution)/shard_map/all_to_all | solution.py:44
  97.9 4.1 %all-gather.3.cloned.1.call-done = bf16[2048,2816]{1,0:T(8,128)(2,1)} async-done(((bf16[32,2816]{1,0:T(8,128)(2,1)}), bf16[2048,2816]{1,0:T(8,128)(2,1)}) %all-gather.3.cloned.1.call-update) | async-done | bytes 11534352 | tf_op jit(solution)/shard_map/all_gather | solution.py:66
  102.0 8.2 %fusion.14 = f32[512,1408]{1,0:T(8,128)} fusion(bf16[512,2048]{1,0:T(8,128)(2,1)} %bitcast.53, bf16[2048,2816]{1,0:T(8,128)(2,1)} %all-gather.3.cloned.1.call-done), kind=kOutput, calls=%fused_computation.25 | convolution fusion | flops 2952790016 | bytes 10747904 | tf_op jit(solution)/shard_map/dot_general | solution.py:152
  110.2 71.3 %all-gather.5.cloned.1.call-done = bf16[1408,2048]{0,1:T(8,128)(2,1)} async-done(((bf16[1408,32]{0,1:T(8,128)(2,1)}), bf16[1408,2048]{0,1:T(8,128)(2,1)}) %all-gather.5.cloned.1.call-update) | async-done | bytes 5767184 | tf_op jit(solution)/shard_map/all_gather | solution.py:101
  181.5 13.8 %convolution_convert_fusion.2 = bf16[512,2048]{1,0:T(8,128)(2,1)} fusion(bf16[1408,2048]{0,1:T(8,128)(2,1)} %all-gather.5.cloned.1.call-done, bf16[512,2048]{1,0:T(8,128)(2,1)} %bitcast.54, bf16[2048,2816]{1,0:T(8,128)(2,1)} %all-gather.3.cloned.1.call-done, f32[512,1408]{1,0:T(8,128)} %fusion.14), kind=kOutput, calls=%fused_computation.31 | convolution fusion | flops 5910953984 | bytes 18612224 | tf_op jit(solution)/shard_map/dot_general | solution.py:158
  195.4 29.0 %reduce-scatter.2.cloned.1.call-done = bf16[128,2048]{1,0:T(8,128)(2,1)} async-done(((bf16[512,2048]{1,0:T(8,128)(2,1)}), bf16[128,2048]{1,0:T(8,128)(2,1)}) %reduce-scatter.2.cloned.1.call-update) | async-done | bytes 524304 | tf_op jit(solution)/shard_map/reduce_scatter | solution.py:157
  224.4 2.2 add_convert_fusion
  (47 shorter events, 2.7 us)
Async XLA Ops:
  6.5 25.6 %copy-start = (bf16[512,2048]{1,0:T(8,128)(2,1)S(1)}, bf16[512,2048]{1,0:T(8,128)(2,1)}, u32[]{:S(2)}) copy-start(bf16[512,2048]{1,0:T(8,128)(2,1)} %param.18) | copy-start | bytes 6291460
  6.5 95.5 %all-gather.3.cloned.1.call-start = ((), (), s32[]{:S(2)}) async-start(), calls=%async_computation.3 | async-start | bytes 11714560 | tf_op jit(solution)/shard_map/all_gather | solution.py:66
  8.3 173.2 %all-gather.5.cloned.1.call-start = ((), (), s32[]{:S(2)}) async-start(), calls=%async_computation.4 | async-start | bytes 5857280 | tf_op jit(solution)/shard_map/all_gather | solution.py:101
  9.9 6.5 %collective-permute-start = (bf16[2,128,128]{2,1,0:T(8,128)(2,1)S(1)}, bf16[2,128,128]{2,1,0:T(8,128)(2,1)S(1)}, u32[]{:S(2)}, u32[]{:S(2)}) collective-permute-start(bf16[2,128,128]{2,1,0:T(8,128)(2,1)S(1)} %get-tuple-element.122), channel_id=1, source_target_pairs={{0,4},{4,8},{8,12},{12,16},{16,20},{20,24},{24,28},{28,32},{32,36}... | collective-permute-start | bytes 196616 | tf_op jit(solution)/shard_map/ppermute | solution.py:22
  14.4 5.6 %collective-permute-start.1 = (bf16[2,128,128]{2,1,0:T(8,128)(2,1)S(1)}, bf16[2,128,128]{2,1,0:T(8,128)(2,1)S(1)}, u32[]{:S(2)}, u32[]{:S(2)}) collective-permute-start(bf16[2,128,128]{2,1,0:T(8,128)(2,1)S(1)} %get-tuple-element.123), channel_id=1, source_target_pairs={{4,0},{8,4},{12,8},{16,12},{20,16},{24,20},{28,24},{32,28},{36,32}... | collective-permute-start | bytes 196616 | tf_op jit(solution)/shard_map/ppermute | solution.py:24
  23.6 0.7 copy-start.2
  24.7 1.0 copy-start.4
  25.8 0.8 copy-start.5
  29.1 0.7 copy-start.2
  30.2 1.0 copy-start.4
  31.3 0.8 copy-start.5
  35.7 29.2 %all-to-all-start = ((bf16[4,128,2048]{2,1,0:T(8,128)(2,1)}), bf16[4,128,2048]{2,1,0:T(8,128)(2,1)}, u32[]{:S(2)}, u32[]{:S(2)}) async-start(bf16[4,128,2048]{2,1,0:T(8,128)(2,1)} %bitcast.52), calls=%async_computation | async-start | bytes 4194304 | tf_op jit(solution)/shard_map/all_to_all | solution.py:38
  40.2 184.2 %reduce-scatter.2.cloned.1.call-start = ((), (), s32[]{:S(2)}) async-start(), calls=%async_computation.5 | async-start | bytes 2621440 | tf_op jit(solution)/shard_map/reduce_scatter | solution.py:157
  40.2 27.2 %copy-start.3 = (f32[2048]{0:T(1024)S(1)}, f32[2048]{0:T(1024)}, u32[]{:S(2)}) copy-start(f32[2048]{0:T(1024)} %param.17) | copy-start | bytes 24580
  64.9 2.2 copy-start.1
Sparse Core Ops, SparseCore 0:
  10.1 91.8 all-gather.2
  104.7 76.7 all-gather.4
  195.5 28.8 reduce-scatter.1
where the time goes:
time: 234 us; the launch traced here: 233 us
  waiting for transfers between devices  133 us (57%)
  blocking collectives  30 us (13%)
  matrix products  27.7 us (12%)
  between operations  13.2 us (6%)
  starting transfers between devices  10.9 us (5%)
  other arithmetic  9.91 us (4%)
  local copies, waits for them, and re-layouts  6.4 us (3%)
    all_gather x1, waiting for transfers between devices, fetch_down(): return lax.all_gather(down_weight, 'sp', axis=1, tiled=True)  71.3 us
    all_to_all x1, blocking collectives, sent_to_all(): lax.all_to_all(jnp.broadcast_to(value[None], (size, *value.shape)), axis,...  30 us
    reduce_scatter x1, waiting for transfers between devices, shards(): lax.psum_scatter(jnp.dot(picked, down_whole, preferred_element_type=jnp.f...  29 us
    all_to_all x1, waiting for transfers between devices, sent_and_summed(): blocks = lax.all_to_all(split_up(value, dim, size), axis, 0, 0, tiled=True)  24.7 us
    dot_general x1, matrix products, shards(): jnp.dot(picked, down_whole, preferred_element_type=jnp.float32)  13.8 us
    dot_general x1, matrix products, shards(): jnp.dot(normed_all, gate_sectioned, preferred_element_type=jnp.float32)  8.23 us
  transfers between devices with their start and end apart: 6, of which 5 were waited for; matrix products, arithmetic and copies ran while one was open for 10% of the time, Pallas kernels for 0%

commit v1 on v0

v1 whole, which is shorter than its diff:
```python
import functools

import jax
import jax.numpy as jnp
from jax import lax
from jax.experimental import pallas as pl
from jax.experimental.pallas import tpu as pltpu
from jax.sharding import PartitionSpec as P

DH = 128
WIN = 128
EPSILON = 1e-06
MASKED = -1e30
ZN, XN, CN = 8, 4, 2
MESH = pl.DeviceIdType.MESH
F32 = jnp.float32
BF16 = jnp.bfloat16
N_COPIES = 192
FIRST_CHUNKS = 4
LAST_CHUNKS = 8


def body(
    seq_len,
    q_ref,
    k_ref,
    v_ref,
    sink_ref,
    res_hbm,
    gain_ref,
    wo_hbm,
    g_ref,
    u_ref,
    d_ref,
    out_ref,
    kbuf,
    vbuf,
    res_ref,
    wo_ref,
    gate,
    up,
    down,
    att,
    first,
    first_relay,
    first_in,
    middle,
    normed,
    hidden,
    last,
    last_relay,
    last_in,
    send_sems,
    recv_sems,
    local_sems,
):
    sp = lax.axis_index("sp")
    y = lax.axis_index("tp")
    n_sp = lax.axis_size("sp")
    c = lax.rem(sp, CN)
    x = lax.rem(lax.div(sp, CN), XN)
    z = lax.div(sp, CN * XN)
    tok = q_ref.shape[0]
    share = tok // 4
    half = share // 2

    def at_z(k):
        return lax.rem(z + (k + ZN), ZN)

    def spot(zz, xx, cc):
        return {"sp": (zz * XN + xx) * CN + cc, "tp": y}

    z_up, z_down = spot(at_z(1), x, c), spot(at_z(-1), x, c)
    x_up = spot(z, lax.rem(x + 1, XN), c)
    x_down = spot(z, lax.rem(x + XN - 1, XN), c)
    twin = spot(z, x, 1 - c)
    y_up = {"sp": sp, "tp": lax.rem(y + 1, 4)}
    y_down = {"sp": sp, "tp": lax.rem(y + 3, 4)}
    y_far = lax.rem(y + 2, 4)
    right = {"sp": lax.rem(sp + 1, n_sp), "tp": y}
    left = {"sp": lax.rem(sp + n_sp - 1, n_sp), "tp": y}

    sent = []

    def push(src, dst, device):
        i = len(sent)
        copy = pltpu.make_async_remote_copy(
            src_ref=src,
            dst_ref=dst,
            send_sem=send_sems.at[i],
            recv_sem=recv_sems.at[i],
            device_id=device,
            device_id_type=MESH,
        )
        copy.start()
        sent.append(copy)
        return copy

    def local(i, src, dst):
        copy = pltpu.make_async_copy(src, dst, local_sems.at[i])
        copy.start()
        return copy

    wo_copy = local(0, wo_hbm, wo_ref)
    res_copy = local(1, res_hbm.at[pl.ds(pl.multiple_of(y * share, share), share)], res_ref)
    k_copy = local(2, k_ref, kbuf.at[pl.ds(WIN, tok)])
    v_copy = local(3, v_ref, vbuf.at[pl.ds(WIN, tok)])
    own = {
        "g": local(4, g_ref, gate.at[z, x, c]),
        "u": local(5, u_ref, up.at[z, x, c]),
        "d": local(6, d_ref, down.at[z, x, c]),
    }

    barrier = pltpu.get_barrier_semaphore()
    peers = (x_up, x_down, z_up, z_down, twin, y_up, y_down, left, right)
    for peer in peers:
        pl.semaphore_signal(barrier, inc=1, device_id=peer, device_id_type=MESH)
    pl.semaphore_wait(barrier, len(peers))

    buffers = {"u": (u_ref, up), "d": (d_ref, down)}
    spots = (0, -1, 1, -2, 2, -3, 3, 4)
    on_z, on_x, relayed, gate_x, gate_z, twins = {}, {}, {}, {}, {}, {"g": [], "u": [], "d": []}
    lo, hi = pl.ds(0, 16), pl.ds(16, 16)

    def halo():
        return (
            push(k_ref.at[pl.ds(tok - WIN, WIN)], kbuf.at[pl.ds(0, WIN)], right),
            push(v_ref.at[pl.ds(tok - WIN, WIN)], vbuf.at[pl.ds(0, WIN)], right),
            push(k_ref.at[pl.ds(0, WIN)], kbuf.at[pl.ds(WIN + tok, WIN)], left),
            push(v_ref.at[pl.ds(0, WIN)], vbuf.at[pl.ds(WIN + tok, WIN)], left),
        )

    def to_twin(name, ref):
        twins[name].append(push(ref, ref, twin))

    def start_z(m):
        source, buf = buffers[m]
        on_z[m, "u", 1] = push(source, buf.at[z, x, c], z_up)
        on_z[m, "d", 1] = push(source, buf.at[z, x, c], z_down)

    def send_x(m, j):
        source, buf = buffers[m]
        k = spots[j]
        zz = at_z(k)
        block = buf.at[zz, x, c]
        if k == 4:
            on_z[m, "u", 4].wait_recv()
            on_z[m, "d", 4].wait_recv()
        elif k:
            way, n = ("u" if k < 0 else "d"), abs(k)
            on_z[m, way, n].wait_recv()
            passed = block if n < 3 else block.at[lo if way == "u" else hi]
            on_z[m, way, n + 1] = push(passed, passed, z_up if way == "u" else z_down)
        source = block if k else source
        on_x[m, j, "u"] = push(source, block, x_up)
        on_x[m, j, "d"] = push(source, block, x_down)

    def relay_x(m, j):
        buf = buffers[m][1]
        zz = at_z(spots[j])
        on_x[m, j, "u"].wait_recv()
        part = buf.at[zz, lax.rem(x + XN - 1, XN), c, lo]
        relayed[m, j, "u"] = push(part, part, x_up)
        on_x[m, j, "d"].wait_recv()
        part = buf.at[zz, lax.rem(x + 1, XN), c, hi]
        relayed[m, j, "d"] = push(part, part, x_down)

    def close_x(m, j):
        if j == 0:
            own[m].wait()
        relayed[m, j, "u"].wait_recv()
        relayed[m, j, "d"].wait_recv()
        to_twin(m, buffers[m][1].at[at_z(spots[j]), :, c])

    def gate_start():
        gate_x["u"] = push(g_ref, gate.at[z, x, c], x_up)
        gate_x["d"] = push(g_ref, gate.at[z, x, c], x_down)

    def gate_relay():
        gate_x["u"].wait_recv()
        part = gate.at[z, lax.rem(x + XN - 1, XN), c, lo]
        gate_x["ru"] = push(part, part, x_up)
        gate_x["d"].wait_recv()
        part = gate.at[z, lax.rem(x + 1, XN), c, hi]
        gate_x["rd"] = push(part, part, x_down)

    def gate_turn():
        own["g"].wait()
        gate_x["ru"].wait_recv()
        gate_x["rd"].wait_recv()
        bundle = gate.at[z, :, c]
        gate_z["u", 1] = push(bundle, bundle, z_up)
        gate_z["d", 1] = push(bundle, bundle, z_down)
        to_twin("g", bundle)

    def gate_step(k):
        if k == 4:
            gate_z["u", 4].wait_recv()
            gate_z["d", 4].wait_recv()
            to_twin("g", gate.at[at_z(4), :, c])
            return
        for way, zz, to in (("u", at_z(-k), z_up), ("d", at_z(k), z_down)):
            gate_z[way, k].wait_recv()
            bundle = gate.at[zz, :, c]
            if k < 3:
                passed = bundle
            else:
                passed = gate.at[zz, pl.ds(0 if way == "u" else 2, 2), c]
            gate_z[way, k + 1] = push(passed, passed, to)
            to_twin("g", bundle)

    offset = sp * tok

    def attend(b):
        keys = kbuf[pl.ds(b * share, share + 2 * WIN), :]
        values = vbuf[pl.ds(b * share, share + 2 * WIN), :]
        span = share + 2 * WIN
        row = lax.broadcasted_iota(jnp.int32, (share, span), 0)
        col = lax.broadcasted_iota(jnp.int32, (share, span), 1)
        gap = col - row
        place = col + (offset + (b * share - WIN))
        kept = (gap >= 0) & (gap <= 2 * WIN) & (place >= 0) & (place < seq_len)
        for h in range(q_ref.shape[1] // DH):
            query = q_ref[pl.ds(b * share, share), pl.ds(h * DH, DH)]
            score = lax.dot_general(
                query, keys, (((1,), (1,)), ((), ())), preferred_element_type=F32
            ) * DH ** (-0.5)
            score = jnp.where(kept, score, MASKED)
            sink = sink_ref[h]
            top = jnp.maximum(jnp.max(score, axis=-1, keepdims=True), sink)
            weight = jnp.exp(score - top)
            total = jnp.sum(weight, axis=-1, keepdims=True) + jnp.exp(sink - top)
            prob = (weight * (1.0 / total)).astype(BF16)
            att[pl.ds(b * share, share), pl.ds(h * DH, DH)] = jnp.dot(
                prob, values, preferred_element_type=F32
            ).astype(BF16)

    def sum_send(n, part, relay, steps):
        steps[n, "ru"] = push(part.at[n, y_far, pl.ds(0, half)], relay.at[0, n], y_up)
        steps[n, "rd"] = push(part.at[n, y_far, pl.ds(half, half)], relay.at[1, n], y_down)

    def sum_pass(n, part, relay, arrived, steps):
        steps[n, "ru"].wait_recv()
        to = lax.rem(y + 1, 4)
        part[n, to, pl.ds(0, half)] = (
            part[n, to, pl.ds(0, half)].astype(F32) + relay[0, n].astype(F32)
        ).astype(BF16)
        steps[n, "u"] = push(part.at[n, to], arrived.at[0, n], y_up)
        steps[n, "rd"].wait_recv()
        to = lax.rem(y + 3, 4)
        part[n, to, pl.ds(half, half)] = (
            part[n, to, pl.ds(half, half)].astype(F32) + relay[1, n].astype(F32)
        ).astype(BF16)
        steps[n, "d"] = push(part.at[n, to], arrived.at[1, n], y_down)

    def sum_take(n, part, arrived, steps):
        steps[n, "u"].wait_recv()
        steps[n, "d"].wait_recv()
        return part[n, y].astype(F32) + arrived[0, n].astype(F32) + arrived[1, n].astype(F32)

    first_steps, last_steps = {}, {}
    width = wo_ref.shape[1] // FIRST_CHUNKS

    def project(n):
        product = jnp.dot(att[...], wo_ref[:, pl.ds(n * width, width)], preferred_element_type=F32)
        first[n] = product.astype(BF16).reshape(4, share, width)
        sum_send(n, first, first_relay, first_steps)

    def pass_first(n):
        sum_pass(n, first, first_relay, first_in, first_steps)

    spread = {}

    def norm():
        res_copy.wait()
        squares = jnp.zeros((share, 1), F32)
        for n in range(FIRST_CHUNKS):
            cols = pl.ds(n * width, width)
            rows = res_ref[:, cols].astype(F32) + sum_take(n, first, first_in, first_steps)
            middle[:, cols] = rows
            squares += jnp.sum(rows * rows, axis=-1, keepdims=True)
        scale = lax.rsqrt(squares * (1.0 / middle.shape[1]) + EPSILON)
        for n in range(FIRST_CHUNKS):
            cols = pl.ds(n * width, width)
            normed[y, :, cols] = (middle[:, cols] * scale * gain_ref[:, cols]).astype(BF16)
        top, low = normed.at[y, pl.ds(0, half)], normed.at[y, pl.ds(half, half)]
        spread["u0"] = push(top, top, y_up)
        spread["d1"] = push(low, low, y_down)
        spread["u1"] = push(low, low, y_up)
        spread["d0"] = push(top, top, y_down)

    def spread_relay():
        spread["u0"].wait_recv()
        part = normed.at[lax.rem(y + 3, 4), pl.ds(0, half)]
        spread["ru"] = push(part, part, y_up)
        spread["d1"].wait_recv()
        part = normed.at[lax.rem(y + 1, 4), pl.ds(half, half)]
        spread["rd"] = push(part, part, y_down)

    def spread_end():
        for name in ("u1", "d0", "ru", "rd"):
            spread[name].wait_recv()

    rows_in = middle.shape[1]

    def expand_cols(cols):
        tokens = normed[...].reshape(tok, rows_in)
        g_acc = jnp.dot(
            tokens, gate[:, :, :, :, cols].reshape(rows_in, cols.size), preferred_element_type=F32
        )
        u_acc = jnp.dot(
            tokens, up[:, :, :, :, cols].reshape(rows_in, cols.size), preferred_element_type=F32
        )
        hidden[:, cols] = (g_acc / (1.0 + jnp.exp(-g_acc)) * u_acc).astype(BF16)

    def expand(first_tile, tiles):
        def step(t, carry):
            expand_cols(pl.ds(pl.multiple_of(t * 256, 256), 256))
            return carry

        lax.fori_loop(first_tile, first_tile + tiles, step, 0)

    def contract(j):
        block = down[at_z(spots[j])].reshape(256, hidden.shape[1])
        product = lax.dot_general(
            hidden[...], block, (((1,), (1,)), ((), ())), preferred_element_type=F32
        )
        last[j] = product.astype(BF16).reshape(4, share, 256)
        sum_send(j, last, last_relay, last_steps)

    def pass_last(j):
        sum_pass(j, last, last_relay, last_in, last_steps)

    def finish(j):
        total = sum_take(j, last, last_in, last_steps)
        cols = pl.ds(pl.multiple_of(at_z(spots[j]) * 256, 256), 256)
        out_ref[:, cols] = (middle[:, cols] + total).astype(BF16)

    halos = halo()
    gate_start()
    start_z("u")
    send_x("u", 0)
    start_z("d")
    k_copy.wait()
    v_copy.wait()
    attend(1)
    gate_relay()
    send_x("u", 1)
    send_x("u", 2)
    attend(2)
    relay_x("u", 0)
    gate_turn()
    for copy in halos:
        copy.wait_recv()
    attend(0)
    send_x("u", 3)
    send_x("u", 4)
    attend(3)
    relay_x("u", 1)
    wo_copy.wait()
    project(0)
    project(1)
    send_x("u", 5)
    send_x("u", 6)
    project(2)
    project(3)
    close_x("u", 0)
    relay_x("u", 2)
    send_x("u", 7)
    send_x("d", 0)
    pass_first(0)
    close_x("u", 1)
    relay_x("u", 3)
    pass_first(1)
    send_x("d", 1)
    close_x("u", 2)
    relay_x("u", 4)
    pass_first(2)
    gate_step(1)
    send_x("d", 2)
    close_x("u", 3)
    relay_x("u", 5)
    pass_first(3)
    send_x("d", 3)
    close_x("u", 4)
    relay_x("u", 6)
    send_x("d", 4)
    close_x("u", 5)
    relay_x("u", 7)
    gate_step(2)
    send_x("d", 5)
    close_x("u", 6)
    relay_x("d", 0)
    norm()
    send_x("d", 6)
    close_x("u", 7)
    relay_x("d", 1)
    send_x("d", 7)
    close_x("d", 0)
    relay_x("d", 2)
    gate_step(3)
    close_x("d", 1)
    relay_x("d", 3)
    spread_relay()
    close_x("d", 2)
    relay_x("d", 4)
    close_x("d", 3)
    relay_x("d", 5)
    gate_step(4)
    for copy in twins["g"] + twins["u"]:
        copy.wait_recv()
    spread_end()
    expand(0, 2)
    close_x("d", 4)
    relay_x("d", 6)
    expand(2, 2)
    close_x("d", 5)
    relay_x("d", 7)
    expand(4, 1)
    expand_cols(pl.ds(1280, 128))
    close_x("d", 6)
    close_x("d", 7)
    for j in range(LAST_CHUNKS):
        twins["d"][j].wait_recv()
        contract(j)
        if j >= 2:
            pass_last(j - 2)
    pass_last(LAST_CHUNKS - 2)
    pass_last(LAST_CHUNKS - 1)
    for j in range(LAST_CHUNKS):
        finish(j)
    for copy in sent:
        copy.wait_send()


def shards(
    queries,
    key_rows,
    value_rows,
    sink_logits,
    residual,
    norm_gain,
    out_weight,
    gate_weight,
    up_weight,
    down_weight,
):
    tok, width = queries.shape
    d = residual.shape[1]
    rows, ff = gate_weight.shape
    share = tok // 4
    whole = pltpu.VMEM((ZN, XN, CN, rows, ff), BF16)
    wide, narrow = d // FIRST_CHUNKS, d // LAST_CHUNKS
    vmem = pl.BlockSpec(memory_space=pltpu.VMEM)
    hbm = pl.BlockSpec(memory_space=pl.ANY)
    smem = pl.BlockSpec(memory_space=pltpu.SMEM)
    return pl.pallas_call(
        functools.partial(body, tok * lax.axis_size("sp")),
        out_shape=jax.ShapeDtypeStruct((share, d), BF16),
        in_specs=[vmem, vmem, vmem, smem, hbm, vmem, hbm, vmem, vmem, vmem],
        out_specs=vmem,
        scratch_shapes=[
            pltpu.VMEM((tok + 2 * WIN, DH), BF16),
            pltpu.VMEM((tok + 2 * WIN, DH), BF16),
            pltpu.VMEM((share, d), BF16),
            pltpu.VMEM((width, d), BF16),
            whole,
            whole,
            whole,
            pltpu.VMEM((tok, width), BF16),
            pltpu.VMEM((FIRST_CHUNKS, 4, share, wide), BF16),
            pltpu.VMEM((2, FIRST_CHUNKS, share // 2, wide), BF16),
            pltpu.VMEM((2, FIRST_CHUNKS, share, wide), BF16),
            pltpu.VMEM((share, d), F32),
            pltpu.VMEM((4, share, d), BF16),
            pltpu.VMEM((tok, ff), BF16),
            pltpu.VMEM((LAST_CHUNKS, 4, share, narrow), BF16),
            pltpu.VMEM((2, LAST_CHUNKS, share // 2, narrow), BF16),
            pltpu.VMEM((2, LAST_CHUNKS, share, narrow), BF16),
            pltpu.SemaphoreType.DMA((N_COPIES,)),
            pltpu.SemaphoreType.DMA((N_COPIES,)),
            pltpu.SemaphoreType.DMA((7,)),
        ],
        compiler_params=pltpu.CompilerParams(
            collective_id=0, has_side_effects=True, vmem_limit_bytes=67043328
        ),
        name="layer",
    )(
        queries,
        key_rows,
        value_rows,
        sink_logits,
        residual,
        norm_gain.reshape(1, d),
        out_weight,
        gate_weight,
        up_weight,
        down_weight.T,
    )


def solution(mesh):
    placed = (
        P("sp", "tp"),
        P("sp", "tp"),
        P("sp", "tp"),
        P("tp"),
        P("sp", None),
        P(),
        P("tp", None),
        P("sp", "tp"),
        P("sp", "tp"),
        P("tp", "sp"),
    )
    return jax.shard_map(
        shards, mesh=mesh, in_specs=placed, out_specs=P(("sp", "tp"), None), check_vma=False
    )
```

time: 234 us -> 103 us (0.44)
  the two profiles are of different devices: /device:TPU:1 before, /device:TPU:8 now
where the time goes in v1:
time: 103 us
  Pallas kernels  101 us (98%)
  local copies, waits for them, and re-layouts  1.88 us (2%)
    pallas_call x1, Pallas kernels, shards(): pl.pallas_call(functools.partial(body, tok * lax.axis_size('sp')), out_sh...  101 us

profile of v1, /device:TPU:8, one launch (start us, length us, event | category | flops | bytes accessed | tf_op | source)
XLA Modules:
  0.0 103.1 jit_solution(12006163503462347476)
XLA Ops:
  0.0 101.2 %layer.1 = bf16[128,2048]{1,0:T(8,128)(2,1)} custom-call(bf16[512,512]{1,0:T(8,128)(2,1)} %q_ref.1, bf16[512,128]{1,0:T(8,128)(2,1)} %k_ref.1, bf16[512,128]{1,0:T(8,128)(2,1)} %v_ref.1, f32[4]{0:T(128)} %sink_ref.1, bf16[512,2048]{1,0:T(8,128)(2,1)} %res_hbm.1, f32[1,2048]{1,0:T(1,128)} %bitcast.3, bf16[512,2048]{1,0:T(8,128)(2,1)} %wo_hbm.1, ...), custom_call_target="tpu_custom_call" | custom-call | tf_op jit(solution)/shard_map/layer/pallas_call | solution.py:457
  101.2 1.9 %copy.12 = bf16[128,2048]{1,0:T(8,128)(2,1)} copy(bf16[128,2048]{1,0:T(8,128)(2,1)} %layer.1) | data formatting | bytes 1048576

commit v2 on v1

v2 whole, which is shorter than its diff:
```python
import functools

import jax
import jax.numpy as jnp
from jax import lax
from jax.experimental import pallas as pl
from jax.experimental.pallas import tpu as pltpu
from jax.sharding import PartitionSpec as P

DH = 128
WIN = 128
EPSILON = 1e-06
MASKED = -1e30
ZN, XN, CN = 8, 4, 2
MESH = pl.DeviceIdType.MESH
F32 = jnp.float32
BF16 = jnp.bfloat16
N_SENT, N_ARRIVING = 31, 90
LAST_CHUNKS = 8


def body(
    seq_len,
    q_hbm,
    k_hbm,
    v_hbm,
    sink_ref,
    res_hbm,
    gain_hbm,
    wo_hbm,
    g_hbm,
    u_hbm,
    d_hbm,
    out_ref,
    q_ref,
    kbuf,
    vbuf,
    res_ref,
    gain_ref,
    wo_ref,
    gate,
    up,
    down,
    att,
    first,
    first_relay,
    first_in,
    middle,
    normed,
    up_acc,
    hidden,
    last,
    last_relay,
    last_in,
    send_sems,
    recv_sems,
    local_sems,
):
    sp = lax.axis_index("sp")
    y = lax.axis_index("tp")
    n_sp = lax.axis_size("sp")
    c = lax.rem(sp, CN)
    x = lax.rem(lax.div(sp, CN), XN)
    z = lax.div(sp, CN * XN)
    tok = q_ref.shape[0]
    share = tok // 4
    half = share // 2
    top, low = pl.ds(0, half), pl.ds(half, half)

    def at_z(k):
        return lax.rem(z + (k + ZN), ZN)

    def at_x(k):
        return lax.rem(x + (k + XN), XN)

    def spot(zz, xx, cc):
        return {"sp": (zz * XN + xx) * CN + cc, "tp": y}

    z_up, z_down = spot(at_z(1), x, c), spot(at_z(-1), x, c)
    x_up, x_down = spot(z, at_x(1), c), spot(z, at_x(-1), c)
    twin = spot(z, x, 1 - c)
    y_up = {"sp": sp, "tp": lax.rem(y + 1, 4)}
    y_down = {"sp": sp, "tp": lax.rem(y + 3, 4)}
    right = {"sp": lax.rem(sp + 1, n_sp), "tp": y}
    left = {"sp": lax.rem(sp + n_sp - 1, n_sp), "tp": y}

    lo, hi = pl.ds(0, 16), pl.ds(16, 16)
    sent, arriving = [], {}
    kinds = {
        "block": (8, lambda n: gate.at[pl.ds(0, n), 0, 0]),
        "part": (8, lambda n: gate.at[pl.ds(0, n), 0, 0, lo]),
        "bundle": (8, lambda n: gate.at[pl.ds(0, n), :, 0]),
        "halo": (4, lambda n: kbuf.at[pl.ds(0, n * WIN)]),
        "rows": (2, lambda n: first.at[0, pl.ds(0, n * half)]),
        "cols": (8, lambda n: last.at[pl.ds(0, n), 0, top]),
    }

    def push(kind, key, src, dst, device):
        groups = [i for i, (of, n) in enumerate(sent) if of == kind and n < kinds[kind][0]]
        if groups:
            i = groups[0]
            sent[i] = (kind, sent[i][1] + 1)
        else:
            i = len(sent)
            sent.append((kind, 1))
        pltpu.make_async_remote_copy(
            src_ref=src,
            dst_ref=dst,
            send_sem=send_sems.at[i],
            recv_sem=recv_sems.at[arriving.setdefault(key, len(arriving))],
            device_id=device,
            device_id_type=MESH,
        ).start()

    def wait_bytes(sem, ref):
        pltpu.make_async_copy(ref, ref, sem).wait()

    def take(key, kind, n):
        wait_bytes(recv_sems.at[arriving[key]], kinds[kind][1](n))

    def wait_sent():
        for i, (kind, n) in enumerate(sent):
            wait_bytes(send_sems.at[i], kinds[kind][1](n))

    def local(i, src, dst):
        copy = pltpu.make_async_copy(src, dst, local_sems.at[i])
        copy.start()
        return copy

    k_copy = local(0, k_hbm, kbuf.at[pl.ds(WIN, tok)])
    v_copy = local(1, v_hbm, vbuf.at[pl.ds(WIN, tok)])
    own_up = local(2, u_hbm, up.at[z, x, c])
    own_gate = local(3, g_hbm, gate.at[z, x, c])
    own_down = local(4, d_hbm, down.at[z, x, c])
    q_copy = local(5, q_hbm, q_ref)
    wo_copy = local(6, wo_hbm, wo_ref)
    res_copy = local(7, res_hbm.at[pl.ds(pl.multiple_of(y * share, share), share)], res_ref)
    gain_copy = local(8, gain_hbm, gain_ref)

    barrier = pltpu.get_barrier_semaphore()
    peers = (x_up, x_down, z_up, z_down, twin, y_up, y_down, left, right)
    for peer in peers:
        pl.semaphore_signal(barrier, inc=1, device_id=peer, device_id_type=MESH)
    pl.semaphore_wait(barrier, len(peers))

    buffers = {"u": up, "d": down}
    spots = (0, -1, 1, -2, 2, -3, 3, 4)

    def halo():
        k_copy.wait()
        v_copy.wait()
        for start, to, device in ((tok, 0, right), (WIN, WIN + tok, left)):
            for ref in (kbuf, vbuf):
                push("halo", "halo", ref.at[pl.ds(start, WIN)], ref.at[pl.ds(to, WIN)], device)

    def wait_halos():
        take("halo", "halo", 4)

    def to_twin(key, ref):
        push("bundle", key, ref, ref, twin)

    def hop(flow, k, block, halves):
        if k:
            take((flow, k), "block", 2 if k < 4 else 1)
        if k < 4:
            for way, zz, to in ((0, at_z(-k), z_up), (1, at_z(k), z_down)):
                ref = block(zz)
                if k == 3:
                    ref = ref.at[halves[way]]
                push("block" if k < 3 else "part", (flow, k + 1), ref, ref, to)

    def z_hop(m, k):
        hop(m, k, lambda zz: buffers[m].at[zz, x, c], (lo, hi))

    def gate_hop(i, k):
        hop(i, k, lambda zz: gate.at[zz, at_x(i), c], (lo, hi))

    def gate_twin(k):
        for kk in sorted({-k, k if k < 4 else -k}):
            to_twin("gt", gate.at[at_z(kk), :, c])

    def along_x(key, block):
        push("block", key, block, block, x_up)
        push("block", key, block, block, x_down)

    def relay_along_x(key, later, line):
        take(key, "block", 2)
        for part, to in ((line.at[at_x(-1), c, lo], x_up), (line.at[at_x(1), c, hi], x_down)):
            push("part", later, part, part, to)

    def send_x(m, j):
        along_x(("x", m, j), buffers[m].at[at_z(spots[j]), x, c])

    def relay_x(m, j):
        relay_along_x(("x", m, j), ("r", m, j), buffers[m].at[at_z(spots[j])])

    def close_x(m, j):
        take(("r", m, j), "block", 1)
        to_twin("ut" if m == "u" else ("dt", j), buffers[m].at[at_z(spots[j]), :, c])

    def gate_start():
        along_x("gx", gate.at[z, x, c])

    def gate_relay():
        relay_along_x("gx", "gr", gate.at[z])

    def gate_close():
        take("gr", "block", 1)

    def wait_twins(name):
        take(name + "t", "bundle", 8)

    offset = sp * tok
    shares = {0: y, 1: lax.rem(y + 1, 4), 2: lax.rem(y + 3, 4), 3: lax.rem(y + 2, 4)}
    late = lax.div(y, 2)
    inner = lax.rem(lax.div(y + 1, 2), 2)

    def attend(b):
        start = pl.multiple_of(b * share, share)
        span = share + 2 * WIN
        keys = kbuf[pl.ds(start, span), :]
        values = vbuf[pl.ds(start, span), :]
        row = lax.broadcasted_iota(jnp.int32, (share, span), 0)
        col = lax.broadcasted_iota(jnp.int32, (share, span), 1)
        gap = col - row
        place = col + (offset + start - WIN)
        kept = (gap >= 0) & (gap <= 2 * WIN) & (place >= 0) & (place < seq_len)
        for h in range(q_ref.shape[1] // DH):
            query = q_ref[pl.ds(start, share), pl.ds(h * DH, DH)]
            score = lax.dot_general(
                query, keys, (((1,), (1,)), ((), ())), preferred_element_type=F32
            ) * DH ** (-0.5)
            score = jnp.where(kept, score, MASKED)
            sink = sink_ref[h]
            most = jnp.maximum(jnp.max(score, axis=-1, keepdims=True), sink)
            weight = jnp.exp(score - most)
            total = jnp.sum(weight, axis=-1, keepdims=True) + jnp.exp(sink - most)
            prob = (weight * (1.0 / total)).astype(BF16)
            att[pl.ds(start, share), pl.ds(h * DH, DH)] = jnp.dot(
                prob, values, preferred_element_type=F32
            ).astype(BF16)

    def attend_early():
        attend(lax.rem(y + 1 + 2 * late, 4))

    def attend_second():
        attend(lax.rem(y + 2 * (1 - inner), 4))

    def attend_third():
        attend(lax.rem(y + 2 * inner, 4))

    def attend_late():
        attend(lax.rem(y + 3 + 2 * late, 4))

    def project(place):
        start = pl.multiple_of(shares[place] * share, share)
        first[place] = jnp.dot(
            att[pl.ds(start, share), :], wo_ref[...], preferred_element_type=F32
        ).astype(BF16)
        if place == 3:
            push("rows", "far", first.at[3, top], first_relay.at[0], y_up)
            push("rows", "far", first.at[3, low], first_relay.at[1], y_down)
        elif place == 1:
            push("rows", "near", first.at[1, low], first_in.at[0, low], y_up)
        elif place == 2:
            push("rows", "near", first.at[2, top], first_in.at[1, top], y_down)

    def pass_first():
        take("far", "rows", 2)
        first[1, top] = (first[1, top].astype(F32) + first_relay[0].astype(F32)).astype(BF16)
        push("rows", "near", first.at[1, top], first_in.at[0, top], y_up)
        first[2, low] = (first[2, low].astype(F32) + first_relay[1].astype(F32)).astype(BF16)
        push("rows", "near", first.at[2, low], first_in.at[1, low], y_down)

    rows_in = middle.shape[1]

    def norm():
        res_copy.wait()
        gain_copy.wait()
        wait_bytes(recv_sems.at[arriving["near"]], first.at[pl.ds(0, 2)])
        squares = jnp.zeros((share, 1), F32)
        width = 512
        for n in range(rows_in // width):
            cols = pl.ds(n * width, width)
            rows = res_ref[:, cols].astype(F32) + (
                first[0, :, cols].astype(F32)
                + first_in[0, :, cols].astype(F32)
                + first_in[1, :, cols].astype(F32)
            )
            middle[:, cols] = rows
            squares += jnp.sum(rows * rows, axis=-1, keepdims=True)
        scale = lax.rsqrt(squares * (1.0 / rows_in) + EPSILON)
        for n in range(rows_in // width):
            cols = pl.ds(n * width, width)
            normed[0, :, cols] = (middle[:, cols] * scale * gain_ref[:, cols]).astype(BF16)
        push("rows", "s0", normed.at[0, top], normed.at[2, top], y_up)
        push("rows", "s0", normed.at[0, low], normed.at[1, low], y_down)
        push("rows", "s1", normed.at[0, low], normed.at[2, low], y_up)
        push("rows", "s1", normed.at[0, top], normed.at[1, top], y_down)

    def spread_relay():
        take("s0", "rows", 2)
        push("rows", "s2", normed.at[2, top], normed.at[3, top], y_up)
        push("rows", "s2", normed.at[1, low], normed.at[3, low], y_down)

    def spread_near():
        take("s1", "rows", 2)

    def spread_far():
        take("s2", "rows", 2)

    def over_tiles(tile, first_tile, tiles, rest):
        def step(t, carry):
            tile(pl.ds(pl.multiple_of(t * 256, 256), 256))
            return carry

        lax.fori_loop(first_tile, first_tile + tiles, step, 0)
        if rest:
            tile(pl.ds(1280, 128))

    def times(weight, place, count, cols):
        return jnp.dot(
            normed[pl.ds(place, count)].reshape(count * share, rows_in),
            weight[:, :, :, :, cols].reshape(rows_in, cols.size),
            preferred_element_type=F32,
        )

    def expand_up(place, count, first_tile, tiles, rest=False):
        def tile(cols):
            up_acc[pl.ds(place * share, count * share), cols] = times(up, place, count, cols)

        over_tiles(tile, first_tile, tiles, rest)

    def expand_gate(place, count, first_tile, tiles, rest=False):
        def tile(cols):
            rows = pl.ds(place * share, count * share)
            g_acc = times(gate, place, count, cols)
            hidden[rows, cols] = (g_acc / (1.0 + jnp.exp(-g_acc)) * up_acc[rows, cols]).astype(BF16)

        over_tiles(tile, first_tile, tiles, rest)

    def contract(j, place, count):
        product = lax.dot_general(
            hidden[pl.ds(place * share, count * share)],
            down[at_z(spots[j])].reshape(256, hidden.shape[1]),
            (((1,), (1,)), ((), ())),
            preferred_element_type=F32,
        )
        last[j, pl.ds(place, count)] = product.astype(BF16).reshape(count, share, 256)

    def send_near(j):
        push("cols", ("e", j), last.at[j, 1, low], last_in.at[0, j, low], y_up)
        push("cols", ("e", j), last.at[j, 2, top], last_in.at[1, j, top], y_down)

    def send_far(j):
        push("cols", ("f", j), last.at[j, 3, top], last_relay.at[0, j], y_up)
        push("cols", ("f", j), last.at[j, 3, low], last_relay.at[1, j], y_down)

    def contract_near(j):
        take(("dt", j), "bundle", 1)
        contract(j, 0, 3)
        send_near(j)

    def contract_far(j):
        contract(j, 3, 1)
        send_far(j)

    def contract_all(j):
        take(("dt", j), "bundle", 1)
        contract(j, 0, 4)
        send_far(j)
        send_near(j)

    def pass_last(j):
        take(("f", j), "cols", 2)
        last[j, 1, top] = (
            last[j, 1, top].astype(F32) + last_relay[0, j].astype(F32)
        ).astype(BF16)
        push("cols", ("e", j), last.at[j, 1, top], last_in.at[0, j, top], y_up)
        last[j, 2, low] = (
            last[j, 2, low].astype(F32) + last_relay[1, j].astype(F32)
        ).astype(BF16)
        push("cols", ("e", j), last.at[j, 2, low], last_in.at[1, j, low], y_down)

    def finish(j):
        take(("e", j), "cols", 4)
        cols = pl.ds(pl.multiple_of(at_z(spots[j]) * 256, 256), 256)
        total = last[j, 0].astype(F32) + last_in[0, j].astype(F32) + last_in[1, j].astype(F32)
        out_ref[:, cols] = (middle[:, cols] + total).astype(BF16)

    halo()
    own_up.wait()
    z_hop("u", 0)
    own_gate.wait()
    gate_start()
    send_x("u", 0)
    gate_hop(0, 0)
    q_copy.wait()
    attend_early()
    own_down.wait()
    z_hop("d", 0)
    attend_second()
    send_x("d", 0)
    wait_halos()
    attend_third()
    wo_copy.wait()
    z_hop("u", 1)
    send_x("u", 1)
    project(3)
    gate_relay()
    gate_hop(1, 0)
    gate_hop(-1, 0)
    attend_late()
    gate_hop(0, 1)
    project(1)
    relay_x("u", 0)
    project(2)
    project(0)
    send_x("u", 2)
    relay_x("d", 0)
    z_hop("u", 2)
    send_x("u", 3)
    relay_x("u", 1)
    gate_close()
    gate_hop(2, 0)
    gate_twin(0)
    gate_hop(1, 1)
    close_x("u", 0)
    pass_first()
    send_x("u", 4)
    gate_hop(-1, 1)
    relay_x("u", 2)
    close_x("d", 0)
    gate_hop(0, 2)
    relay_x("u", 3)
    z_hop("u", 3)
    send_x("u", 5)
    close_x("u", 1)
    send_x("u", 6)
    gate_hop(2, 1)
    gate_twin(1)
    relay_x("u", 4)
    close_x("u", 2)
    gate_hop(1, 2)
    close_x("u", 3)
    gate_hop(-1, 2)
    norm()
    relay_x("u", 5)
    gate_hop(0, 3)
    relay_x("u", 6)
    z_hop("u", 4)
    send_x("u", 7)
    close_x("u", 4)
    z_hop("d", 1)
    send_x("d", 1)
    close_x("u", 5)
    gate_hop(2, 2)
    gate_twin(2)
    send_x("d", 2)
    close_x("u", 6)
    gate_hop(1, 3)
    relay_x("u", 7)
    gate_hop(-1, 3)
    spread_relay()
    gate_hop(0, 4)
    relay_x("d", 1)
    relay_x("d", 2)
    close_x("u", 7)
    gate_hop(2, 3)
    z_hop("d", 2)
    send_x("d", 3)
    send_x("d", 4)
    gate_twin(3)
    close_x("d", 1)
    gate_hop(1, 4)
    spread_near()
    wait_twins("u")
    expand_up(0, 3, 0, 2)
    gate_hop(-1, 4)
    close_x("d", 2)
    expand_up(0, 3, 2, 2)
    gate_hop(2, 4)
    gate_twin(4)
    expand_up(0, 3, 4, 1, True)
    relay_x("d", 3)
    z_hop("d", 3)
    send_x("d", 5)
    send_x("d", 6)
    wait_twins("g")
    expand_gate(0, 3, 0, 2)
    relay_x("d", 4)
    expand_gate(0, 3, 2, 2)
    spread_far()
    expand_up(3, 1, 0, 5, True)
    z_hop("d", 4)
    send_x("d", 7)
    close_x("d", 3)
    expand_gate(0, 3, 4, 1, True)
    relay_x("d", 5)
    contract_near(0)
    contract_near(1)
    relay_x("d", 6)
    contract_near(2)
    expand_gate(3, 1, 0, 5, True)
    close_x("d", 4)
    contract_far(0)
    relay_x("d", 7)
    contract_far(1)
    contract_far(2)
    close_x("d", 5)
    contract_near(3)
    close_x("d", 6)
    contract_far(3)
    contract_all(4)
    pass_last(0)
    close_x("d", 7)
    contract_all(5)
    pass_last(1)
    pass_last(2)
    contract_all(6)
    contract_all(7)
    pass_last(3)
    pass_last(4)
    finish(0)
    pass_last(5)
    finish(1)
    finish(2)
    pass_last(6)
    pass_last(7)
    finish(3)
    finish(4)
    finish(5)
    finish(6)
    finish(7)
    wait_sent()
    assert (len(sent), len(arriving)) == (N_SENT, N_ARRIVING)


def shards(
    queries,
    key_rows,
    value_rows,
    sink_logits,
    residual,
    norm_gain,
    out_weight,
    gate_weight,
    up_weight,
    down_weight,
):
    tok, width = queries.shape
    d = residual.shape[1]
    rows, ff = gate_weight.shape
    share = tok // 4
    whole = pltpu.VMEM((ZN, XN, CN, rows, ff), BF16)
    narrow = d // LAST_CHUNKS
    hbm = pl.BlockSpec(memory_space=pl.ANY)
    smem = pl.BlockSpec(memory_space=pltpu.SMEM)
    return pl.pallas_call(
        functools.partial(body, tok * lax.axis_size("sp")),
        out_shape=pltpu.VMEM((share, d), BF16),
        in_specs=[hbm, hbm, hbm, smem, hbm, hbm, hbm, hbm, hbm, hbm],
        out_specs=pl.BlockSpec(memory_space=pltpu.VMEM),
        scratch_shapes=[
            pltpu.VMEM((tok, width), BF16),
            pltpu.VMEM((tok + 2 * WIN, DH), BF16),
            pltpu.VMEM((tok + 2 * WIN, DH), BF16),
            pltpu.VMEM((share, d), BF16),
            pltpu.VMEM((1, d), F32),
            pltpu.VMEM((width, d), BF16),
            whole,
            whole,
            whole,
            pltpu.VMEM((tok, width), BF16),
            pltpu.VMEM((4, share, d), BF16),
            pltpu.VMEM((2, share // 2, d), BF16),
            pltpu.VMEM((2, share, d), BF16),
            pltpu.VMEM((share, d), F32),
            pltpu.VMEM((4, share, d), BF16),
            pltpu.VMEM((tok, ff), F32),
            pltpu.VMEM((tok, ff), BF16),
            pltpu.VMEM((LAST_CHUNKS, 4, share, narrow), BF16),
            pltpu.VMEM((2, LAST_CHUNKS, share // 2, narrow), BF16),
            pltpu.VMEM((2, LAST_CHUNKS, share, narrow), BF16),
            pltpu.SemaphoreType.DMA((N_SENT,)),
            pltpu.SemaphoreType.DMA((N_ARRIVING,)),
            pltpu.SemaphoreType.DMA((9,)),
        ],
        compiler_params=pltpu.CompilerParams(
            collective_id=0, has_side_effects=True, vmem_limit_bytes=67043328 - 2**19
        ),
        name="layer",
    )(
        queries,
        key_rows,
        value_rows,
        sink_logits,
        residual,
        norm_gain.reshape(1, d),
        out_weight,
        gate_weight,
        up_weight,
        down_weight.T,
    )


def solution(mesh):
    placed = (
        P("sp", "tp"),
        P("sp", "tp"),
        P("sp", "tp"),
        P("tp"),
        P("sp", None),
        P(),
        P("tp", None),
        P("sp", "tp"),
        P("sp", "tp"),
        P("tp", "sp"),
    )
    return jax.shard_map(
        shards, mesh=mesh, in_specs=placed, out_specs=P(("sp", "tp"), None), check_vma=False
    )
```

time: 103 us -> 83.5 us (0.81)
  the two profiles are of different devices: /device:TPU:8 before, /device:TPU:1 now
where the time goes in v2:
time: 83.5 us; the launch traced here: 83.4 us
  Pallas kernels  82.6 us (99%)
    pallas_call x1, Pallas kernels, shards(): pl.pallas_call(functools.partial(body, tok * lax.axis_size('sp')), out_sh...  82.6 us

profile of v2, /device:TPU:1, one launch (start us, length us, event | category | flops | bytes accessed | tf_op | source)
XLA Modules:
  0.0 83.4 jit_solution(4896614417524579157)
XLA Ops:
  0.0 82.6 %layer.1 = bf16[128,2048]{1,0:T(8,128)(2,1)S(1)} custom-call(bf16[512,512]{1,0:T(8,128)(2,1)} %q_hbm.1, bf16[512,128]{1,0:T(8,128)(2,1)} %k_hbm.1, bf16[512,128]{1,0:T(8,128)(2,1)} %v_hbm.1, f32[4]{0:T(128)} %sink_ref.1, bf16[512,2048]{1,0:T(8,128)(2,1)} %res_hbm.1, f32[1,2048]{1,0:T(1,128)} %bitcast.3, bf16[512,2048]{1,0:T(8,128)(2,1)} %wo_hbm.1, ...), custom_call_target="tpu_custom_call" | custom-call | tf_op jit(solution)/shard_map/layer/pallas_call | solution.py:559
  82.6 0.8 copy.12

commit v3 on v2

v3 whole, which is shorter than its diff:
```python
import functools

import jax
import jax.numpy as jnp
from jax import lax
from jax.experimental import pallas as pl
from jax.experimental.pallas import tpu as pltpu
from jax.sharding import PartitionSpec as P

DH = 128
WIN = 128
EPSILON = 1e-06
MASKED = -1e30
ZN, XN, CN = 8, 4, 2
MESH = pl.DeviceIdType.MESH
F32 = jnp.float32
BF16 = jnp.bfloat16
N_SENT, N_ARRIVING = 46, 109
LAST_CHUNKS = 8
DIRECT = 7
TAIL = 128


def body(
    seq_len,
    q_hbm,
    k_hbm,
    v_hbm,
    sink_ref,
    res_hbm,
    gain_hbm,
    wo_hbm,
    g_hbm,
    u_hbm,
    d_hbm,
    out_ref,
    q_ref,
    kbuf,
    vbuf,
    res_ref,
    gain_ref,
    wo_ref,
    gate,
    up,
    down,
    att,
    first,
    first_relay,
    first_in,
    middle,
    normed,
    up_acc,
    hidden,
    last,
    last_relay,
    last_in,
    far_in,
    send_sems,
    recv_sems,
    local_sems,
):
    sp = lax.axis_index("sp")
    y = lax.axis_index("tp")
    n_sp = lax.axis_size("sp")
    c = lax.rem(sp, CN)
    x = lax.rem(lax.div(sp, CN), XN)
    z = lax.div(sp, CN * XN)
    tok = q_ref.shape[0]
    share = tok // 4
    half = share // 2
    part = half // 2
    top, low = pl.ds(0, part), pl.ds(part, part)

    def at_z(k):
        return lax.rem(z + (k + ZN), ZN)

    def at_x(k):
        return lax.rem(x + (k + XN), XN)

    def spot(zz, xx, cc):
        return {"sp": (zz * XN + xx) * CN + cc, "tp": y}

    z_up, z_down = spot(at_z(1), x, c), spot(at_z(-1), x, c)
    x_up, x_down = spot(z, at_x(1), c), spot(z, at_x(-1), c)
    twin = spot(z, x, 1 - c)
    y_up = {"sp": sp, "tp": lax.rem(y + 1, 4)}
    y_down = {"sp": sp, "tp": lax.rem(y + 3, 4)}
    y_far = {"sp": sp, "tp": lax.rem(y + 2, 4)}
    right = {"sp": lax.rem(sp + 1, n_sp), "tp": y}
    left = {"sp": lax.rem(sp + n_sp - 1, n_sp), "tp": y}

    lo, hi = pl.ds(0, 16), pl.ds(16, 16)
    sent, arriving = [], {}
    kinds = {
        "halo": (4, lambda n: kbuf.at[pl.ds(0, n * WIN)]),
        "rows": (2, lambda n: first.at[0, 0, pl.ds(0, n * part)]),
        "cols": (8, lambda n: last.at[pl.ds(0, n), 0, 0, top]),
    }

    for name, ref in (("g", gate), ("u", up), ("d", down)):
        kinds["block", name] = (8, lambda n, ref=ref: ref.at[pl.ds(0, n), 0, 0])
        kinds["part", name] = (8, lambda n, ref=ref: ref.at[pl.ds(0, n), 0, 0, lo])
        kinds["bundle", name] = (8, lambda n, ref=ref: ref.at[pl.ds(0, n), :, 0])

    def push(kind, key, src, dst, device):
        groups = [i for i, (of, n) in enumerate(sent) if of == kind and n < kinds[kind][0]]
        if groups:
            i = groups[0]
            sent[i] = (kind, sent[i][1] + 1)
        else:
            i = len(sent)
            sent.append((kind, 1))
        pltpu.make_async_remote_copy(
            src_ref=src,
            dst_ref=dst,
            send_sem=send_sems.at[i],
            recv_sem=recv_sems.at[arriving.setdefault(key, len(arriving))],
            device_id=device,
            device_id_type=MESH,
        ).start()

    def wait_bytes(sem, ref):
        pltpu.make_async_copy(ref, ref, sem).wait()

    def take(key, kind, n):
        wait_bytes(recv_sems.at[arriving[key]], kinds[kind][1](n))

    def wait_sent():
        for i, (kind, n) in enumerate(sent):
            wait_bytes(send_sems.at[i], kinds[kind][1](n))

    def local(i, src, dst):
        copy = pltpu.make_async_copy(src, dst, local_sems.at[i])
        copy.start()
        return copy

    k_copy = local(0, k_hbm, kbuf.at[pl.ds(WIN, tok)])
    v_copy = local(1, v_hbm, vbuf.at[pl.ds(WIN, tok)])
    ff, cut = u_hbm.shape[1], gate.shape[4]
    own_up = (
        local(2, u_hbm, up.at[z, x, c, :, pl.ds(0, ff)]),
        local(9, g_hbm.at[:, pl.ds(cut, TAIL)], up.at[z, x, c, :, pl.ds(ff, TAIL)]),
    )
    own_gate = local(3, g_hbm.at[:, pl.ds(0, cut)], gate.at[z, x, c])
    own_down = local(4, d_hbm, down.at[z, x, c])
    q_copy = local(5, q_hbm, q_ref)
    wo_copy = local(6, wo_hbm, wo_ref)
    res_copy = local(7, res_hbm.at[pl.ds(pl.multiple_of(y * share, share), share)], res_ref)
    gain_copy = local(8, gain_hbm, gain_ref)

    barrier = pltpu.get_barrier_semaphore()
    peers = (x_up, x_down, z_up, z_down, twin, y_up, y_down, y_far, left, right)
    for peer in peers:
        pl.semaphore_signal(barrier, inc=1, device_id=peer, device_id_type=MESH)
    pl.semaphore_wait(barrier, len(peers))

    buffers = {"u": up, "d": down}
    spots = (0, -1, 1, -2, 2, -3, 3, 4)

    def halo():
        k_copy.wait()
        v_copy.wait()
        for start, to, device in ((tok, 0, right), (WIN, WIN + tok, left)):
            for ref in (kbuf, vbuf):
                push("halo", "halo", ref.at[pl.ds(start, WIN)], ref.at[pl.ds(to, WIN)], device)

    def wait_halos():
        take("halo", "halo", 4)

    def to_twin(m, key, ref):
        push(("bundle", m), key, ref, ref, twin)

    def hop(m, flow, k, block, halves):
        if k:
            take((flow, k), ("block", m), 2 if k < 4 else 1)
        if k < 4:
            for way, zz, to in ((0, at_z(-k), z_up), (1, at_z(k), z_down)):
                ref = block(zz)
                if k == 3:
                    ref = ref.at[halves[way]]
                push(("block" if k < 3 else "part", m), (flow, k + 1), ref, ref, to)

    def z_hop(m, k):
        hop(m, m, k, lambda zz: buffers[m].at[zz, x, c], (lo, hi))

    def gate_hop(i, k):
        hop("g", i, k, lambda zz: gate.at[zz, at_x(i), c], (lo, hi))

    def gate_twin(k):
        for kk in sorted({-k, k if k < 4 else -k}):
            to_twin("g", "gt", gate.at[at_z(kk), :, c])

    def along_x(m, key, block):
        push(("block", m), key, block, block, x_up)
        push(("block", m), key, block, block, x_down)

    def relay_along_x(m, key, later, line):
        take(key, ("block", m), 2)
        for piece, to in ((line.at[at_x(-1), c, lo], x_up), (line.at[at_x(1), c, hi], x_down)):
            push(("part", m), later, piece, piece, to)

    def send_x(m, j):
        along_x(m, ("x", m, j), buffers[m].at[at_z(spots[j]), x, c])

    def relay_x(m, j):
        relay_along_x(m, ("x", m, j), ("r", m, j), buffers[m].at[at_z(spots[j])])

    def close_x(m, j):
        take(("r", m, j), ("block", m), 1)
        to_twin(m, "ut" if m == "u" else ("dt", j), buffers[m].at[at_z(spots[j]), :, c])

    def gate_start():
        along_x("g", "gx", gate.at[z, x, c])

    def gate_relay():
        relay_along_x("g", "gx", "gr", gate.at[z])

    def gate_close():
        take("gr", ("block", "g"), 1)

    def wait_twins(m):
        take(m + "t", ("bundle", m), 8)

    offset = sp * tok
    shares = {0: y, 1: lax.rem(y + 1, 4), 2: lax.rem(y + 3, 4), 3: lax.rem(y + 2, 4)}
    late = lax.div(y, 2)
    inner = lax.rem(lax.div(y + 1, 2), 2)

    def attend(b):
        start = pl.multiple_of(b * share, share)
        span = share + 2 * WIN
        keys = kbuf[pl.ds(start, span), :]
        values = vbuf[pl.ds(start, span), :]
        row = lax.broadcasted_iota(jnp.int32, (share, span), 0)
        col = lax.broadcasted_iota(jnp.int32, (share, span), 1)
        gap = col - row
        place = col + (offset + start - WIN)
        kept = (gap >= 0) & (gap <= 2 * WIN) & (place >= 0) & (place < seq_len)
        for h in range(q_ref.shape[1] // DH):
            query = q_ref[pl.ds(start, share), pl.ds(h * DH, DH)]
            score = lax.dot_general(
                query, keys, (((1,), (1,)), ((), ())), preferred_element_type=F32
            ) * DH ** (-0.5)
            score = jnp.where(kept, score, MASKED)
            sink = sink_ref[h]
            most = jnp.maximum(jnp.max(score, axis=-1, keepdims=True), sink)
            weight = jnp.exp(score - most)
            total = jnp.sum(weight, axis=-1, keepdims=True) + jnp.exp(sink - most)
            prob = (weight * (1.0 / total)).astype(BF16)
            att[pl.ds(start, share), pl.ds(h * DH, DH)] = jnp.dot(
                prob, values, preferred_element_type=F32
            ).astype(BF16)

    def attend_early():
        attend(lax.rem(y + 1 + 2 * late, 4))

    def attend_second():
        attend(lax.rem(y + 2 * (1 - inner), 4))

    def attend_third():
        attend(lax.rem(y + 2 * inner, 4))

    def attend_late():
        attend(lax.rem(y + 3 + 2 * late, 4))

    def project(place):
        start = pl.multiple_of(shares[place] * share, share)
        product = jnp.dot(
            att[pl.ds(start, share), :], wo_ref[...], preferred_element_type=F32
        ).astype(BF16)
        for g in range(2):
            first[g, place] = product[g * half : (g + 1) * half]
        for g in range(2):
            if place == 3:
                push("rows", ("far", g), first.at[g, 3, top], first_relay.at[g, 0], y_up)
                push("rows", ("far", g), first.at[g, 3, low], first_relay.at[g, 1], y_down)

    def first_near(g):
        push("rows", ("near", g), first.at[g, 1, low], first_in.at[g, 0, low], y_up)
        push("rows", ("near", g), first.at[g, 2, top], first_in.at[g, 1, top], y_down)

    def pass_first(g):
        take(("far", g), "rows", 2)
        first[g, 1, top] = (
            first[g, 1, top].astype(F32) + first_relay[g, 0].astype(F32)
        ).astype(BF16)
        push("rows", ("near", g), first.at[g, 1, top], first_in.at[g, 0, top], y_up)
        first[g, 2, low] = (
            first[g, 2, low].astype(F32) + first_relay[g, 1].astype(F32)
        ).astype(BF16)
        push("rows", ("near", g), first.at[g, 2, low], first_in.at[g, 1, low], y_down)

    rows_in = middle.shape[2]

    def norm(g):
        if g == 0:
            res_copy.wait()
            gain_copy.wait()
        wait_bytes(recv_sems.at[arriving["near", g]], first.at[g, pl.ds(0, 2)])
        squares = jnp.zeros((half, 1), F32)
        width = 512
        for n in range(rows_in // width):
            cols = pl.ds(n * width, width)
            rows = res_ref[pl.ds(g * half, half), cols].astype(F32) + (
                first[g, 0, :, cols].astype(F32)
                + first_in[g, 0, :, cols].astype(F32)
                + first_in[g, 1, :, cols].astype(F32)
            )
            middle[g, :, cols] = rows
            squares += jnp.sum(rows * rows, axis=-1, keepdims=True)
        scale = lax.rsqrt(squares * (1.0 / rows_in) + EPSILON)
        for n in range(rows_in // width):
            cols = pl.ds(n * width, width)
            normed[g, 0, :, cols] = (middle[g, :, cols] * scale * gain_ref[:, cols]).astype(BF16)
        push("rows", ("s0", g), normed.at[g, 0, top], normed.at[g, 2, top], y_up)
        push("rows", ("s0", g), normed.at[g, 0, low], normed.at[g, 1, low], y_down)
        push("rows", ("s1", g), normed.at[g, 0, low], normed.at[g, 2, low], y_up)
        push("rows", ("s1", g), normed.at[g, 0, top], normed.at[g, 1, top], y_down)

    def spread_relay(g):
        take(("s0", g), "rows", 2)
        push("rows", ("s2", g), normed.at[g, 2, top], normed.at[g, 3, top], y_up)
        push("rows", ("s2", g), normed.at[g, 1, low], normed.at[g, 3, low], y_down)

    def spread_end(g):
        take(("s1", g), "rows", 2)
        take(("s2", g), "rows", 2)

    def over_tiles(tile, first_tile, tiles):
        def step(t, carry):
            tile(pl.ds(pl.multiple_of(t * 256, 256), 256))
            return carry

        lax.fori_loop(first_tile, first_tile + tiles, step, 0)

    def times(weight, g, cols):
        return jnp.dot(
            normed[g].reshape(tok // 2, rows_in),
            weight[:, :, :, :, cols].reshape(rows_in, cols.size),
            preferred_element_type=F32,
        )

    def expand_up(g, first_tile, tiles):
        def tile(cols):
            up_acc[g, :, cols] = times(up, g, cols)

        over_tiles(tile, first_tile, tiles)

    def open_gate(g, cols, g_acc, u_acc):
        hidden[g, :, cols] = (g_acc / (1.0 + jnp.exp(-g_acc)) * u_acc).astype(BF16)

    def expand_tail(g):
        both = times(up, g, pl.ds(cut, 2 * TAIL))
        open_gate(g, pl.ds(cut, TAIL), both[:, TAIL:], both[:, :TAIL])

    def expand_gate(g, first_tile, tiles):
        def tile(cols):
            open_gate(g, cols, times(gate, g, cols), up_acc[g, :, cols])

        over_tiles(tile, first_tile, tiles)

    def contract(j, g):
        if g == 0:
            take(("dt", j), ("bundle", "d"), 1)
        product = lax.dot_general(
            hidden[g],
            down[at_z(spots[j])].reshape(256, hidden.shape[2]),
            (((1,), (1,)), ((), ())),
            preferred_element_type=F32,
        )
        last[j, g] = product.astype(BF16).reshape(4, half, 256)
        if j >= DIRECT:
            for rows in (top, low):
                push("cols", ("e", j, g), last.at[j, g, 3, rows], far_in.at[j - DIRECT, g, rows], y_far)
                push("cols", ("e", j, g), last.at[j, g, 1, rows], last_in.at[j, g, 0, rows], y_up)
                push("cols", ("e", j, g), last.at[j, g, 2, rows], last_in.at[j, g, 1, rows], y_down)
            return
        push("cols", ("f", j, g), last.at[j, g, 3, top], last_relay.at[j, g, 0], y_up)
        push("cols", ("f", j, g), last.at[j, g, 3, low], last_relay.at[j, g, 1], y_down)
        push("cols", ("e", j, g), last.at[j, g, 1, low], last_in.at[j, g, 0, low], y_up)
        push("cols", ("e", j, g), last.at[j, g, 2, top], last_in.at[j, g, 1, top], y_down)

    def pass_last(j, g):
        take(("f", j, g), "cols", 2)
        last[j, g, 1, top] = (
            last[j, g, 1, top].astype(F32) + last_relay[j, g, 0].astype(F32)
        ).astype(BF16)
        push("cols", ("e", j, g), last.at[j, g, 1, top], last_in.at[j, g, 0, top], y_up)
        last[j, g, 2, low] = (
            last[j, g, 2, low].astype(F32) + last_relay[j, g, 1].astype(F32)
        ).astype(BF16)
        push("cols", ("e", j, g), last.at[j, g, 2, low], last_in.at[j, g, 1, low], y_down)

    def finish(j, g):
        take(("e", j, g), "cols", 6 if j >= DIRECT else 4)
        cols = pl.ds(pl.multiple_of(at_z(spots[j]) * 256, 256), 256)
        total = (
            last[j, g, 0].astype(F32)
            + last_in[j, g, 0].astype(F32)
            + last_in[j, g, 1].astype(F32)
        )
        if j >= DIRECT:
            total += far_in[j - DIRECT, g].astype(F32)
        out_ref[pl.ds(g * half, half), cols] = (middle[g, :, cols] + total).astype(BF16)

    halo()
    for copy in own_up:
        copy.wait()
    z_hop("u", 0)
    own_gate.wait()
    gate_start()
    send_x("u", 0)
    gate_hop(0, 0)
    q_copy.wait()
    attend_early()
    attend_second()
    own_down.wait()
    z_hop("d", 0)
    wait_halos()
    attend_third()
    wo_copy.wait()
    z_hop("u", 1)
    send_x("u", 1)
    send_x("u", 2)
    project(3)
    gate_relay()
    attend_late()
    gate_hop(1, 0)
    project(1)
    relay_x("u", 0)
    gate_hop(-1, 0)
    project(2)
    first_near(0)
    project(0)
    gate_hop(0, 1)
    relay_x("u", 1)
    z_hop("u", 2)
    send_x("u", 3)
    send_x("u", 4)
    relay_x("u", 2)
    gate_close()
    gate_hop(2, 0)
    gate_twin(0)
    pass_first(0)
    first_near(1)
    close_x("u", 0)
    pass_first(1)
    gate_hop(1, 1)
    close_x("u", 1)
    gate_hop(-1, 1)
    relay_x("u", 3)
    z_hop("u", 3)
    send_x("u", 5)
    send_x("u", 6)
    relay_x("u", 4)
    norm(0)
    gate_hop(0, 2)
    close_x("u", 2)
    close_x("u", 3)
    gate_hop(2, 1)
    gate_twin(1)
    gate_hop(1, 2)
    relay_x("u", 5)
    z_hop("u", 4)
    send_x("u", 7)
    gate_hop(-1, 2)
    relay_x("u", 6)
    close_x("u", 4)
    gate_hop(0, 3)
    close_x("u", 5)
    send_x("d", 0)
    spread_relay(0)
    norm(1)
    gate_hop(2, 2)
    gate_twin(2)
    z_hop("d", 1)
    send_x("d", 1)
    relay_x("u", 7)
    close_x("u", 6)
    gate_hop(1, 3)
    gate_hop(-1, 3)
    gate_hop(0, 4)
    send_x("d", 2)
    relay_x("d", 0)
    spread_end(0)
    gate_hop(2, 3)
    gate_twin(3)
    relay_x("d", 1)
    close_x("u", 7)
    z_hop("d", 2)
    spread_relay(1)
    send_x("d", 3)
    gate_hop(1, 4)
    relay_x("d", 2)
    gate_hop(-1, 4)
    wait_twins("u")
    expand_up(0, 0, 3)
    gate_hop(2, 4)
    gate_twin(4)
    close_x("d", 0)
    expand_up(0, 3, 2)
    expand_tail(0)
    send_x("d", 4)
    close_x("d", 1)
    z_hop("d", 3)
    wait_twins("g")
    expand_gate(0, 0, 2)
    spread_end(1)
    relay_x("d", 3)
    expand_gate(0, 2, 3)
    send_x("d", 5)
    close_x("d", 2)
    contract(0, 0)
    contract(1, 0)
    z_hop("d", 4)
    expand_up(1, 0, 3)
    relay_x("d", 4)
    contract(2, 0)
    send_x("d", 6)
    close_x("d", 3)
    expand_up(1, 3, 2)
    expand_tail(1)
    pass_last(0, 0)
    expand_gate(1, 0, 2)
    pass_last(1, 0)
    relay_x("d", 5)
    expand_gate(1, 2, 3)
    pass_last(2, 0)
    send_x("d", 7)
    close_x("d", 4)
    contract(3, 0)
    contract(0, 1)
    contract(1, 1)
    relay_x("d", 6)
    contract(2, 1)
    contract(4, 0)
    close_x("d", 5)
    contract(3, 1)
    pass_last(3, 0)
    contract(4, 1)
    pass_last(0, 1)
    finish(0, 0)
    finish(1, 0)
    finish(2, 0)
    relay_x("d", 7)
    pass_last(1, 1)
    contract(5, 0)
    pass_last(2, 1)
    close_x("d", 6)
    contract(5, 1)
    pass_last(4, 0)
    pass_last(3, 1)
    finish(3, 0)
    pass_last(4, 1)
    close_x("d", 7)
    contract(6, 0)
    contract(6, 1)
    pass_last(5, 0)
    finish(0, 1)
    finish(1, 1)
    finish(2, 1)
    contract(7, 0)
    pass_last(5, 1)
    contract(7, 1)
    finish(4, 0)
    finish(3, 1)
    finish(4, 1)
    pass_last(6, 0)
    pass_last(6, 1)
    finish(5, 0)
    finish(7, 0)
    finish(5, 1)
    finish(7, 1)
    finish(6, 0)
    finish(6, 1)
    wait_sent()
    assert (len(sent), len(arriving)) == (N_SENT, N_ARRIVING)


def shards(
    queries,
    key_rows,
    value_rows,
    sink_logits,
    residual,
    norm_gain,
    out_weight,
    gate_weight,
    up_weight,
    down_weight,
):
    tok, width = queries.shape
    d = residual.shape[1]
    rows, ff = gate_weight.shape
    share = tok // 4
    half = share // 2
    gate_part, up_part, down_part = (
        pltpu.VMEM((ZN, XN, CN, rows, columns), BF16) for columns in (ff - TAIL, ff + TAIL, ff)
    )
    narrow = d // LAST_CHUNKS
    hbm = pl.BlockSpec(memory_space=pl.ANY)
    smem = pl.BlockSpec(memory_space=pltpu.SMEM)
    return pl.pallas_call(
        functools.partial(body, tok * lax.axis_size("sp")),
        out_shape=pltpu.VMEM((share, d), BF16),
        in_specs=[hbm, hbm, hbm, smem, hbm, hbm, hbm, hbm, hbm, hbm],
        out_specs=pl.BlockSpec(memory_space=pltpu.VMEM),
        scratch_shapes=[
            pltpu.VMEM((tok, width), BF16),
            pltpu.VMEM((tok + 2 * WIN, DH), BF16),
            pltpu.VMEM((tok + 2 * WIN, DH), BF16),
            pltpu.VMEM((share, d), BF16),
            pltpu.VMEM((1, d), F32),
            pltpu.VMEM((width, d), BF16),
            gate_part,
            up_part,
            down_part,
            pltpu.VMEM((tok, width), BF16),
            pltpu.VMEM((2, 4, half, d), BF16),
            pltpu.VMEM((2, 2, half // 2, d), BF16),
            pltpu.VMEM((2, 2, half, d), BF16),
            pltpu.VMEM((2, half, d), F32),
            pltpu.VMEM((2, 4, half, d), BF16),
            pltpu.VMEM((2, tok // 2, ff - TAIL), F32),
            pltpu.VMEM((2, tok // 2, ff), BF16),
            pltpu.VMEM((LAST_CHUNKS, 2, 4, half, narrow), BF16),
            pltpu.VMEM((LAST_CHUNKS, 2, 2, half // 2, narrow), BF16),
            pltpu.VMEM((LAST_CHUNKS, 2, 2, half, narrow), BF16),
            pltpu.VMEM((LAST_CHUNKS - DIRECT, 2, half, narrow), BF16),
            pltpu.SemaphoreType.DMA((N_SENT,)),
            pltpu.SemaphoreType.DMA((N_ARRIVING,)),
            pltpu.SemaphoreType.DMA((10,)),
        ],
        compiler_params=pltpu.CompilerParams(
            collective_id=0, has_side_effects=True, vmem_limit_bytes=67043328 - 2**19
        ),
        name="layer",
    )(
        queries,
        key_rows,
        value_rows,
        sink_logits,
        residual,
        norm_gain.reshape(1, d),
        out_weight,
        gate_weight,
        up_weight,
        down_weight.T,
    )


def solution(mesh):
    placed = (
        P("sp", "tp"),
        P("sp", "tp"),
        P("sp", "tp"),
        P("tp"),
        P("sp", None),
        P(),
        P("tp", None),
        P("sp", "tp"),
        P("sp", "tp"),
        P("tp", "sp"),
    )
    return jax.shard_map(
        shards, mesh=mesh, in_specs=placed, out_specs=P(("sp", "tp"), None), check_vma=False
    )
```

time: 83.5 us -> 80.1 us (0.959)
  Pallas kernels: 82.6 us -> 79.2 us
    pallas_call x1, Pallas kernels: 82.6 us -> 79.2 us  [shards(): pl.pallas_call(functools.partial(body, tok * lax.axis_size('sp')), out_sh...]
where the time goes in v3:
time: 80.1 us; the launch traced here: 80 us
  Pallas kernels  79.2 us (99%)
    pallas_call x1, Pallas kernels, shards(): pl.pallas_call(functools.partial(body, tok * lax.axis_size('sp')), out_sh...  79.2 us

profile of v3, /device:TPU:1, one launch (start us, length us, event | category | flops | bytes accessed | tf_op | source)
XLA Modules:
  0.0 80.0 jit_solution(9410792874522291868)
XLA Ops:
  0.0 79.2 %layer.1 = bf16[128,2048]{1,0:T(8,128)(2,1)S(1)} custom-call(bf16[512,512]{1,0:T(8,128)(2,1)} %q_hbm.1, bf16[512,128]{1,0:T(8,128)(2,1)} %k_hbm.1, bf16[512,128]{1,0:T(8,128)(2,1)} %v_hbm.1, f32[4]{0:T(128)} %sink_ref.1, bf16[512,2048]{1,0:T(8,128)(2,1)} %res_hbm.1, f32[1,2048]{1,0:T(1,128)} %bitcast.3, bf16[512,2048]{1,0:T(8,128)(2,1)} %wo_hbm.1, ...), custom_call_target="tpu_custom_call" | custom-call | tf_op jit(solution)/shard_map/layer/pallas_call | solution.py:603
  79.2 0.8 copy.12

commit v4 on v3

--- a/solution.py
+++ b/solution.py
@@ -15,9 +15,10 @@
 MESH = pl.DeviceIdType.MESH
 F32 = jnp.float32
 BF16 = jnp.bfloat16
-N_SENT, N_ARRIVING = 46, 109
+N_SENT, N_ARRIVING = 48, 109
 LAST_CHUNKS = 8
 DIRECT = 7
+PIECES = 5
 TAIL = 128
 
 
@@ -203,10 +204,19 @@
         along_x(m, ("x", m, j), buffers[m].at[at_z(spots[j]), x, c])
 
     def relay_x(m, j):
-        relay_along_x(m, ("x", m, j), ("r", m, j), buffers[m].at[at_z(spots[j])])
+        line = buffers[m].at[at_z(spots[j])]
+        relay_along_x(m, ("x", m, j), ("r", m, j), line)
+        if m == "d" and j >= PIECES:
+            for k in (0, -1, 1):
+                block = line.at[at_x(k), c]
+                push(("block", m), ("dt", j), block, block, twin)
 
     def close_x(m, j):
         take(("r", m, j), ("block", m), 1)
+        if m == "d" and j >= PIECES:
+            block = buffers[m].at[at_z(spots[j]), at_x(2), c]
+            push(("block", m), ("dt", j), block, block, twin)
+            return
         to_twin(m, "ut" if m == "u" else ("dt", j), buffers[m].at[at_z(spots[j]), :, c])
 
     def gate_start():

time: 80.1 us -> 80 us (level)
  no operation moved by 1% of the time
where the time goes in v4:
time: 80 us; the launch traced here: 79.9 us
  Pallas kernels  79.1 us (99%)
  local copies, waits for them, and re-layouts  0.8 us (1%)
    pallas_call x1, Pallas kernels, shards(): pl.pallas_call(functools.partial(body, tok * lax.axis_size('sp')), out_sh...  79.1 us

profile of v4, /device:TPU:1, one launch (start us, length us, event | category | flops | bytes accessed | tf_op | source)
XLA Modules:
  0.0 79.9 jit_solution(11344630603451733870)
XLA Ops:
  0.0 79.1 %layer.1 = bf16[128,2048]{1,0:T(8,128)(2,1)S(1)} custom-call(bf16[512,512]{1,0:T(8,128)(2,1)} %q_hbm.1, bf16[512,128]{1,0:T(8,128)(2,1)} %k_hbm.1, bf16[512,128]{1,0:T(8,128)(2,1)} %v_hbm.1, f32[4]{0:T(128)} %sink_ref.1, bf16[512,2048]{1,0:T(8,128)(2,1)} %res_hbm.1, f32[1,2048]{1,0:T(1,128)} %bitcast.3, bf16[512,2048]{1,0:T(8,128)(2,1)} %wo_hbm.1, ...), custom_call_target="tpu_custom_call" | custom-call | tf_op jit(solution)/shard_map/layer/pallas_call | solution.py:613
  79.1 0.8 copy.12
